TPU v7x, 32 devices: a whole 2x2x4 slice. The times are simulated.
32 devices in a mesh: kv: 8 (over z, y), tp: 4 (over x, core).
Axes of the slice: x: 2, y: 2, z: 4, core: 2. Of those that a mesh axis runs over, the one named last changes fastest.
Arguments:
- hidden_in: bfloat16 [16, 4096], P(None, ('kv', 'tp')), may hold values from -12 to 12
- attn_gain: float32 [4096], P('kv'), may hold values from 0.1 to 1.9
- query_weight: bfloat16 [4096, 4096], P('kv', 'tp'), may hold values from -0.09375 to 0.09375
- key_cache: bfloat16 [16, 8192, 8, 128], P(None, 'kv', 'tp'), may hold values from -600 to 600
- value_cache: bfloat16 [16, 8192, 8, 128], P(None, 'kv', 'tp'), may hold values from -6 to 6
- lambdas: float32 [32], P('tp'), may hold values from 0.3 to 0.8
- head_gain: float32 [128], replicated, may hold values from 0.1 to 1.9
- out_weight: bfloat16 [4096, 4096], P('tp', 'kv'), may hold values from -0.09375 to 0.09375
- mixer_gain: float32 [4096], P(('kv', 'tp')), may hold values from 0.1 to 1.9
- gate_weight: bfloat16 [4096, 11264], P('kv', 'tp'), may hold values from -0.09375 to 0.09375
- up_weight: bfloat16 [4096, 11264], P('kv', 'tp'), may hold values from -0.09375 to 0.09375
- down_weight: bfloat16 [11264, 4096], P('tp', 'kv'), may hold values from -0.0546875 to 0.0546875
Outputs:
- mixed: bfloat16 [16, 4096], P(None, ('kv', 'tp'))
All inputs are finite; a program needn't handle non-finite values.
Results may differ from a plain program's by a relative error of at most 0.017.
Values may be sent and summed in bfloat16 or wider, within the bound.
A program may use at most 64 MiB of HBM per device.

v0:
```python
import jax
import jax.numpy as jnp
from jax import lax
from jax.sharding import PartitionSpec as P

D = 4096
HEAD_DIM = 64


eps = 1e-06


def finish_heads(totals, weighted, lambdas, head_gain, kv_dev, group_size):
    head_means = weighted / totals[..., None]
    mixing = lambdas.reshape(kv_dev, group_size)
    attended = head_means[0] - mixing[None, :, :, None] * head_means[1]
    norm_inv = lax.rsqrt(jnp.mean(attended * attended, axis=-1, keepdims=True) + eps)
    head_out = (attended * norm_inv * head_gain).astype(jnp.bfloat16)
    return head_out.reshape(head_out.shape[0], kv_dev * group_size * 2 * HEAD_DIM)


def per_device(
    hidden_in,
    attn_gain,
    query_weight,
    key_cache,
    value_cache,
    lambdas,
    head_gain,
    out_weight,
    mixer_gain,
    gate_weight,
    up_weight,
    down_weight,
):
    batch_rows = hidden_in.shape[0]
    rows_block = lax.all_gather(hidden_in, "tp", axis=1, tiled=True)
    block_f = rows_block.astype(jnp.float32)
    gained = (block_f * attn_gain).astype(jnp.bfloat16)
    partial_value = jnp.dot(gained, query_weight, preferred_element_type=jnp.float32)
    own_cols = hidden_in.astype(jnp.float32)
    squares = lax.psum(jnp.sum(own_cols * own_cols, axis=1), ("kv", "tp"))
    query_full = lax.psum(partial_value, "kv")
    row_scale = lax.rsqrt(squares / D + eps)
    query_rows = (query_full * row_scale[:, None]).astype(jnp.bfloat16)
    positions = key_cache.shape[1]
    kv_dev = key_cache.shape[2]
    heads_dev = query_rows.shape[1] // (2 * HEAD_DIM)
    group_size = heads_dev // kv_dev
    query_heads = query_rows.reshape(batch_rows, kv_dev, group_size, 2, HEAD_DIM)
    key_rows = key_cache.reshape(batch_rows, positions, kv_dev, 2, HEAD_DIM)
    scores = jnp.einsum(
        "bkgcd,bpkcd->cbkgp", query_heads, key_rows, preferred_element_type=jnp.float32
    ) * HEAD_DIM ** (-0.5)
    maxima = jnp.max(scores, axis=-1)
    exponent = jnp.exp(scores - maxima[..., None])
    totals = jnp.sum(exponent, axis=-1)
    exp_weights = exponent.astype(jnp.bfloat16)
    weighted = jnp.einsum(
        "cbkgp,bpkv->cbkgv", exp_weights, value_cache, preferred_element_type=jnp.float32
    )
    parts_max, parts_tot, parts_acc = (
        lax.all_to_all(maxima[None], "kv", split_axis=2, concat_axis=0, tiled=True),
        lax.all_to_all(totals[None], "kv", split_axis=2, concat_axis=0, tiled=True),
        lax.all_to_all(weighted[None], "kv", split_axis=2, concat_axis=0, tiled=True),
    )
    top = jnp.max(parts_max, axis=0)
    factors = jnp.exp(parts_max - top[None])
    own_tot = jnp.sum(parts_tot * factors, axis=0)
    own_acc = jnp.sum(parts_acc * factors[..., None], axis=0)
    own_out = finish_heads(own_tot, own_acc, lambdas, head_gain, kv_dev, group_size)
    head_out = lax.all_gather(own_out, "kv", axis=0, tiled=True)
    projected = jnp.dot(head_out, out_weight, preferred_element_type=jnp.float32)
    attn_out = lax.psum_scatter(
        projected.astype(jnp.bfloat16), "tp", scatter_dimension=1, tiled=True
    ).astype(jnp.float32)
    after_attn = (hidden_in.astype(jnp.float32) + attn_out).astype(jnp.bfloat16)
    after_f = after_attn.astype(jnp.float32)
    squares_two = lax.psum(jnp.sum(after_f * after_f, axis=1), ("kv", "tp"))
    mixer_in = (after_f * lax.rsqrt(squares_two / D + eps)[:, None] * mixer_gain).astype(
        jnp.bfloat16
    )
    gathered = lax.all_gather(mixer_in, "tp", axis=1, tiled=True)
    gate_part = jnp.dot(gathered, gate_weight, preferred_element_type=jnp.float32)
    up_part = jnp.dot(gathered, up_weight, preferred_element_type=jnp.float32)
    gate_sum, up_sum = lax.psum((gate_part, up_part), "kv")
    hidden = (jax.nn.silu(gate_sum) * up_sum).astype(jnp.bfloat16)
    down_part = jnp.dot(hidden, down_weight, preferred_element_type=jnp.float32)
    mixer_out = lax.psum_scatter(
        down_part.astype(jnp.bfloat16), "tp", scatter_dimension=1, tiled=True
    ).astype(jnp.float32)
    return (after_f + mixer_out).astype(jnp.bfloat16)


def solution(mesh):
    in_specs = (
        P(None, ("kv", "tp")),
        P("kv"),
        P("kv", "tp"),
        P(None, "kv", "tp", None),
        P(None, "kv", "tp", None),
        P("tp"),
        P(),
        P("tp", "kv"),
        P(("kv", "tp")),
        P("kv", "tp"),
        P("kv", "tp"),
        P("tp", "kv"),
    )
    out_specs = P(None, ("kv", "tp"))
    return jax.shard_map(
        per_device, mesh=mesh, in_specs=in_specs, out_specs=out_specs, check_vma=False
    )
```

profile of v0, /device:TPU:0, one launch (start us, length us, event | category | flops | bytes accessed | tf_op | source)
XLA Modules:
  0.0 329.5 jit_solution(1171620726180046008)
XLA Ops:
  6.5 6.5 %all_gather.9 = bf16[16,512]{1,0:T(8,128)(2,1)S(1)} all-gather(bf16[16,128]{1,0:T(8,128)(2,1)} %param.12), channel_id=1, replica_groups=mesh['kv'=8,'tp'=4] {'tp'}, dimensions={1}, use_global_device_ids=true | all-gather | bytes 20480 | tf_op jit(solution)/shard_map/all_gather | solution.py:37
  13.0 0.8 fusion.17
  13.8 2.1 fusion.15
  16.0 41.0 %psum.36 = f32[16]{0:T(128)S(1)} all-reduce(f32[16]{0:T(128)S(1)} %fusion.17), channel_id=1, replica_groups=mesh['kv'=8,'tp'=4] {'kv','tp'}, use_global_device_ids=true, to_apply=%region_2.0 | all-reduce | flops 16 | bytes 128 | tf_op jit(solution)/shard_map/psum | solution.py:42
  57.0 21.2 %copy.33 = bf16[16,1024,2,128]{1,3,2,0:T(8,128)(2,1)} copy(bf16[16,1024,2,128]{3,2,1,0:T(2,128)(2,1)} %param.15) | data formatting | bytes 16777216 | tf_op args[3]
  78.2 9.0 %all-reduce.4.cloned.1.call-done = f32[16,1024]{1,0:T(8,128)} async-done(((f32[16,1024]{1,0:T(8,128)}), f32[16,1024]{1,0:T(8,128)}) %all-reduce.4.cloned.1.call-update) | async-done | bytes 65552 | tf_op jit(solution)/shard_map/psum | solution.py:43
  87.1 0.9 multiply_convert_fusion.2
  88.1 0.1 reshape.35
  88.2 4.7 %fusion.28 = (f32[2,16,2,4]{3,2,1,0:T(2,128)S(1)}, f32[2,16,2,4,1024]{4,3,2,1,0:T(4,128)S(1)}) fusion(bf16[16,1024,2,2,64]{1,4,3,2,0:T(8,128)(2,1)} %bitcast.56, bf16[16,2,4,2,64]{4,3,2,1,0:T(2,128)(2,1)S(1)} %reshape.35), kind=kOutput, calls=%fused_computation.46 | convolution fusion | flops 34078464 | bytes 9470976 | tf_op jit(solution)/shard_map/bkgcd,bpkcd->cbkgp/dot_general | solution.py:52
  92.9 0.6 fusion.10
  93.5 0.6 copy.41
  94.1 4.5 %all-to-all-start.2 = ((f32[1,2,16,2,4]{4,3,1,0,2:T(2,128)}), f32[1,2,16,2,4]{4,3,1,0,2:T(2,128)S(1)}, u32[]{:S(2)}, u32[]{:S(2)}) async-start(f32[1,2,16,2,4]{4,3,1,0,2:T(2,128)} %copy.41), calls=%async_computation.2 | async-start | bytes 65536 | tf_op jit(solution)/shard_map/all_to_all | solution.py:64
  98.6 0.6 copy.39
  99.3 6.1 %all-to-all-done.2 = f32[1,2,16,2,4]{4,3,1,0,2:T(2,128)S(1)} async-done(((f32[1,2,16,2,4]{4,3,1,0,2:T(2,128)}), f32[1,2,16,2,4]{4,3,1,0,2:T(2,128)S(1)}, u32[]{:S(2)}, u32[]{:S(2)}) %all-to-all-start.2) | async-done | bytes 1056 | tf_op jit(solution)/shard_map/all_to_all | solution.py:64
  105.3 3.3 %all-to-all-start.1 = ((f32[1,2,16,2,4]{4,3,1,0,2:T(2,128)}), f32[1,2,16,2,4]{4,3,1,0,2:T(2,128)S(1)}, u32[]{:S(2)}, u32[]{:S(2)}) async-start(f32[1,2,16,2,4]{4,3,1,0,2:T(2,128)} %copy.39), calls=%async_computation.1 | async-start | bytes 65536 | tf_op jit(solution)/shard_map/all_to_all | solution.py:63
  108.7 5.5 %fusion.7 = f32[1,2,16,2,4,128]{5,4,1,3,0,2:T(4,128)} fusion(bf16[16,1024,2,128,1]{3,2,1,0,4:T(2,128)(2,1)} %bitcast.69, bf16[2,16,2,4,1024]{4,3,2,1,0:T(4,128)(2,1)S(1)} %get-tuple-element.10), kind=kOutput, calls=%fused_computation.5 | convolution fusion | flops 67108864 | bytes 9043968 | tf_op jit(solution)/shard_map/cbkgp,bpkv->cbkgv/dot_general | solution.py:59
  114.2 1.1 all-to-all-done.1
  115.3 4.8 %all-to-all-start = ((f32[1,2,16,2,4,128]{5,4,1,3,0,2:T(4,128)}), f32[1,2,16,2,4,128]{5,4,1,3,0,2:T(4,128)S(1)}, u32[]{:S(2)}, u32[]{:S(2)}) async-start(f32[1,2,16,2,4,128]{5,4,1,3,0,2:T(4,128)} %fusion.7), calls=%async_computation | async-start | bytes 262144 | tf_op jit(solution)/shard_map/all_to_all | solution.py:65
  120.1 0.0 reduce-scatter.7.cloned.1.call-start
  120.2 0.1 mul.118
  120.3 0.1 multiply_reduce_fusion.1
  120.4 7.1 %all-to-all-done = f32[1,2,16,2,4,128]{5,4,1,3,0,2:T(4,128)S(1)} async-done(((f32[1,2,16,2,4,128]{5,4,1,3,0,2:T(4,128)}), f32[1,2,16,2,4,128]{5,4,1,3,0,2:T(4,128)S(1)}, u32[]{:S(2)}, u32[]{:S(2)}) %all-to-all-start) | async-done | bytes 131104 | tf_op jit(solution)/shard_map/all_to_all | solution.py:65
  127.5 0.1 multiply_reduce_fusion
  127.6 0.1 broadcast_divide_fusion
  127.8 0.2 fusion.24
  127.9 0.1 mul.126
  128.0 0.1 mul.119
  128.1 30.6 %all-gather = bf16[8,2,1024]{2,1,0:T(2,128)(2,1)S(1)} all-gather(bf16[1,2,1024]{2,1,0:T(2,128)(2,1)S(1)} %fusion.25), channel_id=1, replica_groups=mesh['kv'=8,'tp'=4] {'kv'}, dimensions={0}, use_global_device_ids=true | all-gather | bytes 36864 | tf_op jit(solution)/shard_map/all_gather | solution.py:72
  158.8 1.5 convolution_convert_fusion.1
  160.2 0.8 copy.47
  161.0 0.0 all-reduce.6.cloned.1.call-start
  161.1 17.5 %reduce-scatter.7.cloned.1.call-done = bf16[128,16]{1,0:T(8,128)(2,1)} async-done(((bf16[512,16]{1,0:T(8,128)(2,1)}), bf16[128,16]{1,0:T(8,128)(2,1)}) %reduce-scatter.7.cloned.1.call-update) | async-done | bytes 4112
  178.6 0.8 copy.48
  179.4 0.1 fusion.19
  179.5 39.3 %psum.37 = f32[16]{0:T(128)S(1)} all-reduce(f32[16]{0:T(128)S(1)} %fusion.19), channel_id=1, replica_groups=mesh['kv'=8,'tp'=4] {'kv','tp'}, use_global_device_ids=true, to_apply=%region_11.0 | all-reduce | flops 16 | bytes 128 | tf_op jit(solution)/shard_map/psum | solution.py:79
  218.8 0.1 fusion.21
  218.9 5.6 %all_gather.11 = bf16[16,512]{1,0:T(8,128)(2,1)S(1)} all-gather(bf16[16,128]{1,0:T(8,128)(2,1)S(1)} %fusion.21), channel_id=1, replica_groups=mesh['kv'=8,'tp'=4] {'tp'}, dimensions={1}, use_global_device_ids=true | all-gather | bytes 20480 | tf_op jit(solution)/shard_map/all_gather | solution.py:83
  224.5 1.2 fusion.29
  225.6 1.2 fusion.30
  226.8 0.0 all-reduce.6.cloned.1.call-update
  226.8 0.0 reduce-scatter.9.cloned.1.call-start
  226.9 72.3 %all-reduce.6.cloned.1.call-done = (f32[16,2816]{1,0:T(8,128)}, f32[16,2816]{1,0:T(8,128)}) async-done(((f32[16,2816]{1,0:T(8,128)}, f32[16,2816]{1,0:T(8,128)}), (f32[16,2816]{1,0:T(8,128)}, f32[16,2816]{1,0:T(8,128)})) %all-reduce.6.cloned.1.call-update) | async-done | bytes 360464 | tf_op jit(solution)/shard_map/psum | solution.py:86
  299.2 2.5 convolution_convert_fusion
  301.7 0.7 copy.49
  302.4 0.0 reduce-scatter.9.cloned.1.call-update
  302.5 19.1 %reduce-scatter.9.cloned.1.call-done = bf16[128,16]{1,0:T(8,128)(2,1)} async-done(((bf16[512,16]{1,0:T(8,128)(2,1)}), bf16[128,16]{1,0:T(8,128)(2,1)}) %reduce-scatter.9.cloned.1.call-update) | async-done | bytes 4112
  321.6 0.8 copy.50
  322.4 0.6 fusion.22
  (28 shorter events, 0.2 us)
Async XLA Ops:
  6.5 217.9 %copy-start = (bf16[512,2816]{1,0:T(8,128)(2,1)S(1)}, bf16[512,2816]{1,0:T(8,128)(2,1)}, u32[]{:S(2)}) copy-start(bf16[512,2816]{1,0:T(8,128)(2,1)} %param.21) | copy-start | bytes 8650756
  6.5 80.6 %all-reduce.4.cloned.1.call-start = ((), (), s32[]{:S(2)}) async-start(), calls=%async_computation.5 | async-start | bytes 131072 | tf_op jit(solution)/shard_map/psum | solution.py:43
  94.1 11.2 %all-to-all-start.2 = ((f32[1,2,16,2,4]{4,3,1,0,2:T(2,128)}), f32[1,2,16,2,4]{4,3,1,0,2:T(2,128)S(1)}, u32[]{:S(2)}, u32[]{:S(2)}) async-start(f32[1,2,16,2,4]{4,3,1,0,2:T(2,128)} %copy.41), calls=%async_computation.2 | async-start | bytes 65536 | tf_op jit(solution)/shard_map/all_to_all | solution.py:64
  105.3 10.0 %all-to-all-start.1 = ((f32[1,2,16,2,4]{4,3,1,0,2:T(2,128)}), f32[1,2,16,2,4]{4,3,1,0,2:T(2,128)S(1)}, u32[]{:S(2)}, u32[]{:S(2)}) async-start(f32[1,2,16,2,4]{4,3,1,0,2:T(2,128)} %copy.39), calls=%async_computation.1 | async-start | bytes 65536 | tf_op jit(solution)/shard_map/all_to_all | solution.py:63
  108.7 11.5 %copy-start.5 = (f32[8]{0:T(128)S(1)}, f32[8]{0:T(128)}, u32[]{:S(2)}) copy-start(f32[8]{0:T(128)} %param.17) | copy-start | bytes 100
  108.7 19.4 %copy-start.3 = (f32[128]{0:T(128)S(1)}, f32[128]{0:T(128)}, u32[]{:S(2)}) copy-start(f32[128]{0:T(128)} %param.18) | copy-start | bytes 1540
  108.7 70.7 %copy-start.2 = (bf16[16,128]{1,0:T(8,128)(2,1)S(1)}, bf16[16,128]{1,0:T(8,128)(2,1)}, u32[]{:S(2)}) copy-start(bf16[16,128]{1,0:T(8,128)(2,1)} %param.12) | copy-start | bytes 12292
  108.7 110.1 %copy-start.4 = (f32[128]{0:T(128)S(1)}, f32[128]{0:T(128)}, u32[]{:S(2)}) copy-start(f32[128]{0:T(128)} %param.20) | copy-start | bytes 1540
  115.3 12.2 %all-to-all-start = ((f32[1,2,16,2,4,128]{5,4,1,3,0,2:T(4,128)}), f32[1,2,16,2,4,128]{5,4,1,3,0,2:T(4,128)S(1)}, u32[]{:S(2)}, u32[]{:S(2)}) async-start(f32[1,2,16,2,4,128]{5,4,1,3,0,2:T(4,128)} %fusion.7), calls=%async_computation | async-start | bytes 262144 | tf_op jit(solution)/shard_map/all_to_all | solution.py:65
  120.1 58.4 %reduce-scatter.7.cloned.1.call-start = ((), (), s32[]{:S(2)}) async-start(), calls=%async_computation.6 | async-start | bytes 163840
  161.0 138.2 %all-reduce.6.cloned.1.call-start = ((), (), s32[]{:S(2)}) async-start(), calls=%async_computation.8 | async-start | bytes 720896 | tf_op jit(solution)/shard_map/psum | solution.py:86
  218.8 6.8 %copy-start.1 = (bf16[512,2816]{1,0:T(8,128)(2,1)S(1)}, bf16[512,2816]{1,0:T(8,128)(2,1)}, u32[]{:S(2)}) copy-start(bf16[512,2816]{1,0:T(8,128)(2,1)} %param.22) | copy-start | bytes 8650756
  226.8 94.8 %reduce-scatter.9.cloned.1.call-start = ((), (), s32[]{:S(2)}) async-start(), calls=%async_computation.7 | async-start | bytes 163840
Sparse Core Ops, SparseCore 0:
  16.1 71.0 all-reduce.3
  161.1 17.3 reduce-scatter.6
  226.9 72.2 all-reduce.5
  302.6 18.9 reduce-scatter.8
where the time goes:
time: 331 us; the launch traced here: 330 us
  waiting for transfers between devices  132 us (40%)
  blocking collectives  123 us (37%)
  local copies, waits for them, and re-layouts  26 us (8%)
  matrix products  18.6 us (6%)
  between operations  13.3 us (4%)
  starting transfers between devices  12.8 us (4%)
  other arithmetic  3.66 us (1%)
    psum x1, waiting for transfers between devices, per_device(): gate_sum, up_sum = lax.psum((gate_part, up_part), 'kv')  72.3 us
    psum x1, blocking collectives, per_device(): squares = lax.psum(jnp.sum(own_cols * own_cols, axis=1), ('kv', 'tp'))  41 us
    psum x1, blocking collectives, per_device(): squares_two = lax.psum(jnp.sum(after_f * after_f, axis=1), ('kv', 'tp'))  39.3 us
    unnamed x6, waiting for transfers between devices  36.7 us
    all_gather x1, blocking collectives, per_device(): head_out = lax.all_gather(own_out, 'kv', axis=0, tiled=True)  30.6 us
    unnamed x18, local copies, waits for them, and re-layouts  24.3 us
    psum x1, waiting for transfers between devices, per_device(): query_full = lax.psum(partial_value, 'kv')  8.99 us
    all_to_all x1, waiting for transfers between devices, per_device(): lax.all_to_all(weighted[None], 'kv', split_axis=2, concat_axis=0, tiled=T...  7.09 us
  transfers between devices with their start and end apart: 7, of which 7 were waited for; matrix products, arithmetic and copies ran while one was open for 8% of the time, Pallas kernels for 0%

commit v1 on v0

--- a/solution.py
+++ b/solution.py
@@ -1,13 +1,369 @@
+import functools
+import math
+
 import jax
 import jax.numpy as jnp
 from jax import lax
+from jax.experimental import pallas as pl
+from jax.experimental.pallas import tpu as pltpu
 from jax.sharding import PartitionSpec as P
 
-D = 4096
+MESH = pl.DeviceIdType.MESH
+F32, BF16 = jnp.float32, jnp.bfloat16
+eps = 1e-06
+LANES = 128
+CHUNKS = 4
+NT = (((1,), (1,)), ((), ()))
+
+
+def fused_kernel(
+    cfg,
+    hidden_ref, again_ref, lam_ref, hgain_ref, mgain_ref,
+    wq_hbm, k_hbm, v_hbm, wo_hbm, wg_hbm, wu_hbm, wd_hbm,
+    out_ref,
+    wq, kc, vc, wo, wg, wu, wd,
+    xg, gsend, gainb, qs, qr, sqs, sqr, qown, qg, qall,
+    acc_s, stat_s, accb, statb, accr, statr,
+    hown, hg, ps, pr, aown, ag, sq2s, sq2r, gus, gur, hid_own, hid,
+    local_sem, kv_sem, send_kv, recv_kv, send_tp, recv_tp,
+):
+    n_kv, n_tp, width, head_dim, group, kv_dev = cfg
+    batch = hidden_ref.shape[0]
+    cols = hidden_ref.shape[1]
+    half = batch // 2
+    heads = n_kv
+    me = lax.axis_index("kv")
+    mt = lax.axis_index("tp")
+    per = batch // CHUNKS
+    slope = head_dim ** -0.5 * math.log2(math.e)
+
+    ff = wg_hbm.shape[1]
+    ff_pad = wg.shape[1]
+    piece = ff_pad // n_kv
+
+    def local(i, src, dst):
+        return pltpu.make_async_copy(src, dst, local_sem.at[i])
+
+    c_wq = local(0, wq_hbm, wq)
+    c_wo = local(1, wo_hbm, wo)
+    c_wg = local(2, wg_hbm, wg.at[:, pl.ds(0, ff)])
+    c_wu = local(3, wu_hbm, wu.at[:, pl.ds(0, ff)])
+    c_wd = local(4, wd_hbm, wd.at[pl.ds(0, ff), :])
+
+    def cache_copy(which, hbm, vm, i):
+        return pltpu.make_async_copy(
+            hbm.at[pl.ds(i * per, per)], vm.at[pl.ds(i * per, per)], kv_sem.at[which, i]
+        )
+
+    c_wq.start()
+    for i in range(CHUNKS):
+        cache_copy(0, k_hbm, kc, i).start()
+        cache_copy(1, v_hbm, vc, i).start()
+    c_wo.start()
+    c_wg.start()
+    c_wu.start()
+    c_wd.start()
+
+    barrier = pltpu.get_barrier_semaphore()
+    for d in range(1, n_kv):
+        pl.semaphore_signal(
+            barrier, inc=1, device_id={"kv": lax.rem(me + d, n_kv)}, device_id_type=MESH
+        )
+    for d in range(1, n_tp):
+        pl.semaphore_signal(
+            barrier, inc=1, device_id={"tp": lax.rem(mt + d, n_tp)}, device_id_type=MESH
+        )
+
+    if ff_pad > ff:
+        zc = jnp.zeros((wg.shape[0], ff_pad - ff), BF16)
+        wg[:, ff:] = zc
+        wu[:, ff:] = zc
+        wd[ff:, :] = jnp.zeros((ff_pad - ff, wd.shape[1]), BF16)
+    gsend[...] = jnp.broadcast_to(mgain_ref[...], gsend.shape)
+    pl.semaphore_wait(barrier, n_kv - 1 + n_tp - 1)
+
+    def kv_copy(phase, d, src, dst):
+        return pltpu.make_async_remote_copy(
+            src_ref=src, dst_ref=dst,
+            send_sem=send_kv.at[phase, d], recv_sem=recv_kv.at[phase, d],
+            device_id={"kv": lax.rem(me + d, n_kv)}, device_id_type=MESH,
+        )
+
+    def tp_copy(phase, d, src, dst):
+        return pltpu.make_async_remote_copy(
+            src_ref=src, dst_ref=dst,
+            send_sem=send_tp.at[phase, d], recv_sem=recv_tp.at[phase, d],
+            device_id={"tp": lax.rem(mt + d, n_tp)}, device_id_type=MESH,
+        )
+
+    sent = []
+
+    def to_kv(phase, pick_src, pick_dst):
+        started = []
+        for d in range(1, n_kv):
+            peer = lax.rem(me + d, n_kv)
+            c = kv_copy(phase, d, pick_src(d, peer), pick_dst(d))
+            c.start()
+            started.append(c)
+        sent.extend(started)
+        return started
+
+    def to_tp(phase, pick_src, pick_dst):
+        started = []
+        for d in range(1, n_tp):
+            peer = lax.rem(mt + d, n_tp)
+            c = tp_copy(phase, d, pick_src(d, peer), pick_dst(d))
+            c.start()
+            started.append(c)
+        sent.extend(started)
+        return started
+
+    def arrive(copies):
+        for c in copies:
+            c.wait_recv()
+
+    lane8 = lax.broadcasted_iota(jnp.int32, (half, LANES), 1)
+
+    def pack_rows(sq):
+        return jnp.where(
+            lane8 < LANES // 2,
+            jnp.broadcast_to(sq[:half], (half, LANES)),
+            jnp.broadcast_to(sq[half:], (half, LANES)),
+        )
+
+    def unpack_rows(s):
+        return jnp.concatenate([s[:, 0:1], s[:, LANES // 2 : LANES // 2 + 1]], axis=0)
+
+    cx = to_tp(0, lambda d, p: hidden_ref, lambda d: xg.at[mt])
+    cgain = to_tp(1, lambda d, p: gsend, lambda d: gainb.at[mt])
+    xg[mt] = hidden_ref[...]
+    gainb[mt] = gsend[...]
+    arrive(cx)
+    xf = jnp.concatenate([xg[t] for t in range(n_tp)], axis=1).astype(F32)
+    gained = (xf * again_ref[...]).astype(BF16)
+    sqs[...] = pack_rows(jnp.sum(xf * xf, axis=1, keepdims=True))
+    csq = to_kv(0, lambda d, p: sqs, lambda d: sqr.at[d])
+
+    c_wq.wait()
+    qp = jnp.dot(gained, wq[...], preferred_element_type=F32)
+    hw = 2 * head_dim
+    for j in range(heads):
+        qs[j] = qp[:, j * hw : (j + 1) * hw]
+    cq = to_kv(1, lambda d, p: qs.at[p], lambda d: qr.at[d])
+    arrive(csq)
+    sq = sqs[...]
+    for d in range(1, n_kv):
+        sq = sq + sqr[d]
+    scale1 = lax.rsqrt(unpack_rows(sq) / width + eps)
+    q = qs[me]
+    for d, c in enumerate(cq, 1):
+        c.wait_recv()
+        q = q + qr[d]
+    qown[...] = (q * scale1).astype(BF16)
+    cqg = to_kv(2, lambda d, p: qown, lambda d: qg.at[me])
+    qg[me] = qown[...]
+    lane16 = lax.broadcasted_iota(jnp.int32, (batch, hw), 1)
+    arrive(cqg)
+    for j in range(heads):
+        qj = qg[j].astype(F32)
+        for c in range(2):
+            r = 2 * j + c
+            keep = (lane16 // head_dim) == c
+            qall[r * batch : (r + 1) * batch, :] = jnp.where(keep, qj, 0.0)
+
+    rows = 2 * heads
+    flat = kc.shape[1]
+    row_i = lax.broadcasted_iota(jnp.int32, (rows, flat), 0)
+    lane_i = lax.broadcasted_iota(jnp.int32, (rows, flat), 1)
+    own_key = lax.rem(lane_i, kv_dev) == row_i // (2 * group)
+    lane_r = lax.broadcasted_iota(jnp.int32, (rows, LANES), 1)
+    is_max = lax.rem(lane_r, LANES // 2) < LANES // 4
+
+    def attend(i, carry):
+        cache_copy(0, k_hbm, kc, i).wait()
+        cache_copy(1, v_hbm, vc, i).wait()
+        for u in range(per):
+            b = i * per + u
+            qb = qall[pl.ds(b, rows, stride=batch), :].astype(BF16)
+            s = lax.dot_general(qb, kc[b], NT, preferred_element_type=F32)
+            s = jnp.where(own_key, s, -jnp.inf)
+            m = jnp.max(s, axis=1, keepdims=True)
+            p = jnp.exp2((s - m) * slope)
+            t = jnp.sum(p, axis=1, keepdims=True)
+            a = jnp.dot(p.astype(BF16), vc[b], preferred_element_type=F32)
+            acc_s[pl.ds(b, rows, stride=batch), :] = a
+            stat_s[pl.ds(b, rows, stride=batch), :] = jnp.where(
+                is_max, jnp.broadcast_to(m, (rows, LANES)), jnp.broadcast_to(t, (rows, LANES))
+            )
+        return carry
+
+    lax.fori_loop(0, CHUNKS, attend, 0)
+
+    lane_b = lax.broadcasted_iota(jnp.int32, (batch, LANES), 1)
+    for j in range(heads):
+        lo = 2 * j * batch
+        accb[j] = acc_s[lo : lo + 2 * batch, :].astype(BF16)
+        statb[j] = jnp.where(
+            lane_b < LANES // 2, stat_s[lo : lo + batch, :], stat_s[lo + batch : lo + 2 * batch, :]
+        )
+    cst = to_kv(3, lambda d, p: statb.at[p], lambda d: statr.at[d])
+    cac = to_kv(4, lambda d, p: accb.at[p], lambda d: accr.at[d])
+    statr[0] = statb[me]
+    accr[0] = accb[me]
+    arrive(cst)
+    quarter = LANES // 4
+    means = []
+    factors = []
+    totals = []
+    for c in range(2):
+        base = c * (LANES // 2)
+        ms = [statr[d][:, base : base + 1] for d in range(n_kv)]
+        ts = [statr[d][:, base + quarter : base + quarter + 1] for d in range(n_kv)]
+        top = functools.reduce(jnp.maximum, ms)
+        fs = [jnp.exp2((m - top) * slope) for m in ms]
+        totals.append(functools.reduce(jnp.add, [t * f for t, f in zip(ts, fs)]))
+        factors.append(fs)
+    arrive(cac)
+    for c in range(2):
+        num = functools.reduce(
+            jnp.add,
+            [accr[d][c * batch : (c + 1) * batch].astype(F32) * factors[c][d] for d in range(n_kv)],
+        )
+        means.append(num / totals[c])
+    attended = means[0] - lam_ref[me] * means[1]
+    norm_inv = lax.rsqrt(jnp.mean(attended * attended, axis=-1, keepdims=True) + eps)
+    hown[...] = (attended * norm_inv * hgain_ref[...]).astype(BF16)
+
+    chg = to_kv(5, lambda d, p: hown, lambda d: hg.at[me])
+    hg[me] = hown[...]
+    c_wo.wait()
+    arrive(chg)
+    ho = jnp.concatenate([hg[j] for j in range(heads)], axis=1)
+    proj = jnp.dot(ho, wo[...], preferred_element_type=F32).astype(BF16)
+    for t in range(n_tp):
+        ps[0, t] = proj[:, t * cols : (t + 1) * cols]
+    cp = to_tp(2, lambda d, p: ps.at[0, p], lambda d: pr.at[0, d])
+    attn = ps[0, mt].astype(F32)
+    for d, c in enumerate(cp, 1):
+        c.wait_recv()
+        attn = attn + pr[0, d].astype(F32)
+    aown[...] = (hidden_ref[...].astype(F32) + attn).astype(BF16)
+
+    ca = to_tp(3, lambda d, p: aown, lambda d: ag.at[mt])
+    ag[mt] = aown[...]
+    arrive(cgain)
+    gain = jnp.concatenate([gainb[t][0:1] for t in range(n_tp)], axis=1)
+    arrive(ca)
+    af = jnp.concatenate([ag[t] for t in range(n_tp)], axis=1).astype(F32)
+    mixin = (af * gain).astype(BF16)
+    sq2s[...] = pack_rows(jnp.sum(af * af, axis=1, keepdims=True))
+    csq2 = to_kv(6, lambda d, p: sq2s, lambda d: sq2r.at[d])
+    c_wg.wait()
+    c_wu.wait()
+    cgu = []
+    for d in list(range(1, n_kv)) + [0]:
+        peer = lax.rem(me + d, n_kv)
+        at = pl.ds(pl.multiple_of(peer * piece, LANES), piece)
+        gp = jnp.dot(mixin, wg[:, at], preferred_element_type=F32)
+        up = jnp.dot(mixin, wu[:, at], preferred_element_type=F32)
+        if d == 0:
+            gate_sum, up_sum = gp, up
+        else:
+            gus[d, 0] = gp.astype(BF16)
+            gus[d, 1] = up.astype(BF16)
+            c = kv_copy(7, d, gus.at[d], gur.at[d])
+            c.start()
+            cgu.append(c)
+    sent.extend(cgu)
+    arrive(csq2)
+    sq = sq2s[...]
+    for d in range(1, n_kv):
+        sq = sq + sq2r[d]
+    scale2 = lax.rsqrt(unpack_rows(sq) / width + eps)
+    for d, c in enumerate(cgu, 1):
+        c.wait_recv()
+        gate_sum = gate_sum + gur[d, 0].astype(F32)
+        up_sum = up_sum + gur[d, 1].astype(F32)
+    gate_sum = gate_sum * scale2
+    up_sum = up_sum * scale2
+    hid_own[...] = (gate_sum / (1.0 + jnp.exp(-gate_sum)) * up_sum).astype(BF16)
+    chid = to_kv(8, lambda d, p: hid_own, lambda d: hid.at[me])
+    c_wd.wait()
+    at0 = pl.ds(pl.multiple_of(me * piece, LANES), piece)
+    down = jnp.dot(hid_own[...], wd[at0, :], preferred_element_type=F32)
+    for d, c in enumerate(chid, 1):
+        c.wait_recv()
+        src = lax.rem(me + n_kv - d, n_kv)
+        at = pl.ds(pl.multiple_of(src * piece, LANES), piece)
+        down = down + jnp.dot(hid[src], wd[at, :], preferred_element_type=F32)
+    downb = down.astype(BF16)
+    for t in range(n_tp):
+        ps[1, t] = downb[:, t * cols : (t + 1) * cols]
+    cd = to_tp(4, lambda d, p: ps.at[1, p], lambda d: pr.at[1, d])
+    mix = ps[1, mt].astype(F32)
+    for d, c in enumerate(cd, 1):
+        c.wait_recv()
+        mix = mix + pr[1, d].astype(F32)
+    out_ref[...] = (aown[...].astype(F32) + mix).astype(BF16)
+    for c in sent:
+        c.wait_send()
+
+
+def fused(n_kv, n_tp, hidden_in, attn_gain, query_weight, key_cache, value_cache, lambdas,
+          head_gain, out_weight, mixer_gain, gate_weight, up_weight, down_weight):
+    batch, cols = hidden_in.shape
+    positions, kv_dev, hw = key_cache.shape[1:]
+    heads = lambdas.shape[0]
+    group = heads // kv_dev
+    width = cols * n_kv * n_tp
+    block, ff = gate_weight.shape
+    piece = -(-ff // (LANES * n_kv)) * LANES
+    ff_pad = piece * n_kv
+    keys = key_cache.reshape(batch, positions * kv_dev, hw)
+    values = value_cache.reshape(batch, positions * kv_dev, hw)
+    half = batch // 2
+    V = pltpu.VMEM
+    scratch = [
+        V(query_weight.shape, BF16), V(keys.shape, BF16), V(values.shape, BF16),
+        V(out_weight.shape, BF16), V((block, ff_pad), BF16), V((block, ff_pad), BF16),
+        V((ff_pad, down_weight.shape[1]), BF16),
+        V((n_tp, batch, cols), BF16), V((8, cols), F32), V((n_tp, 8, cols), F32),
+        V((heads, batch, hw), F32), V((n_kv, batch, hw), F32),
+        V((half, LANES), F32), V((n_kv, half, LANES), F32),
+        V((batch, hw), BF16), V((heads, batch, hw), BF16), V((2 * heads * batch, hw), F32),
+        V((2 * heads * batch, hw), F32), V((2 * heads * batch, LANES), F32),
+        V((heads, 2 * batch, hw), BF16), V((heads, batch, LANES), F32),
+        V((n_kv, 2 * batch, hw), BF16), V((n_kv, batch, LANES), F32),
+        V((batch, hw), BF16), V((heads, batch, hw), BF16),
+        V((2, n_tp, batch, cols), BF16), V((2, n_tp, batch, cols), BF16),
+        V((batch, cols), BF16), V((n_tp, batch, cols), BF16),
+        V((half, LANES), F32), V((n_kv, half, LANES), F32),
+        V((n_kv, 2, batch, piece), BF16), V((n_kv, 2, batch, piece), BF16),
+        V((batch, piece), BF16), V((n_kv, batch, piece), BF16),
+        pltpu.SemaphoreType.DMA((5,)), pltpu.SemaphoreType.DMA((2, CHUNKS)),
+        pltpu.SemaphoreType.DMA((9, n_kv)), pltpu.SemaphoreType.DMA((9, n_kv)),
+        pltpu.SemaphoreType.DMA((5, n_tp)), pltpu.SemaphoreType.DMA((5, n_tp)),
+    ]
+    vmem = pl.BlockSpec(memory_space=pltpu.VMEM)
+    smem = pl.BlockSpec(memory_space=pltpu.SMEM)
+    hbm = pl.BlockSpec(memory_space=pl.ANY)
+    cfg = (n_kv, n_tp, width, hw // 2, group, kv_dev)
+    return pl.pallas_call(
+        functools.partial(fused_kernel, cfg),
+        out_shape=jax.ShapeDtypeStruct((batch, cols), BF16),
+        in_specs=[vmem, vmem, smem, vmem, vmem] + [hbm] * 7,
+        out_specs=vmem,
+        scratch_shapes=scratch,
+        compiler_params=pltpu.CompilerParams(
+            collective_id=0, has_side_effects=True, vmem_limit_bytes=60 * 1024 * 1024
+        ),
+    )(
+        hidden_in, attn_gain.reshape(1, block), lambdas, head_gain.reshape(1, hw),
+        mixer_gain.reshape(1, cols), query_weight, keys, values, out_weight,
+        gate_weight, up_weight, down_weight,
+    )
+
 HEAD_DIM = 64
-
-
-eps = 1e-06
 
 
 def finish_heads(totals, weighted, lambdas, head_gain, kv_dev, group_size):
@@ -34,6 +390,7 @@
     down_weight,
 ):
     batch_rows = hidden_in.shape[0]
+    width = hidden_in.shape[1] * lax.axis_size(("kv", "tp"))
     rows_block = lax.all_gather(hidden_in, "tp", axis=1, tiled=True)
     block_f = rows_block.astype(jnp.float32)
     gained = (block_f * attn_gain).astype(jnp.bfloat16)
@@ -41,7 +398,7 @@
     own_cols = hidden_in.astype(jnp.float32)
     squares = lax.psum(jnp.sum(own_cols * own_cols, axis=1), ("kv", "tp"))
     query_full = lax.psum(partial_value, "kv")
-    row_scale = lax.rsqrt(squares / D + eps)
+    row_scale = lax.rsqrt(squares / width + eps)
     query_rows = (query_full * row_scale[:, None]).astype(jnp.bfloat16)
     positions = key_cache.shape[1]
     kv_dev = key_cache.shape[2]
@@ -77,7 +434,7 @@
     after_attn = (hidden_in.astype(jnp.float32) + attn_out).astype(jnp.bfloat16)
     after_f = after_attn.astype(jnp.float32)
     squares_two = lax.psum(jnp.sum(after_f * after_f, axis=1), ("kv", "tp"))
-    mixer_in = (after_f * lax.rsqrt(squares_two / D + eps)[:, None] * mixer_gain).astype(
+    mixer_in = (after_f * lax.rsqrt(squares_two / width + eps)[:, None] * mixer_gain).astype(
         jnp.bfloat16
     )
     gathered = lax.all_gather(mixer_in, "tp", axis=1, tiled=True)
@@ -93,6 +450,14 @@
 
 
 def solution(mesh):
+    n_kv, n_tp = mesh.shape["kv"], mesh.shape["tp"]
+
+    def layer(*arrays):
+        heads_dev = arrays[5].shape[0]
+        if heads_dev == n_kv:
+            return fused(n_kv, n_tp, *arrays)
+        return per_device(*arrays)
+
     in_specs = (
         P(None, ("kv", "tp")),
         P("kv"),
@@ -109,5 +474,5 @@
     )
     out_specs = P(None, ("kv", "tp"))
     return jax.shard_map(
-        per_device, mesh=mesh, in_specs=in_specs, out_specs=out_specs, check_vma=False
-    )
+        layer, mesh=mesh, in_specs=in_specs, out_specs=out_specs, check_vma=False
+    )

time: 331 us -> 59.2 us (0.18)
  waiting for transfers between devices: 132 us -> 0 us
  blocking collectives: 123 us -> 0 us
  Pallas kernels: 0 us -> 57.8 us
  local copies, waits for them, and re-layouts: 26 us -> 1.28 us
  matrix products: 18.6 us -> 0 us
  between operations: 13.3 us -> 0.01 us
  starting transfers between devices: 12.8 us -> 0 us
  other arithmetic: 3.66 us -> 0 us
    psum x2 -> x0, waiting for transfers between devices: 81.3 us -> none  [the longest x1 72.3 us: per_device(): gate_sum, up_sum = lax.psum((gate_part, up_part), 'kv')]
    psum x2 -> x0, blocking collectives: 80.3 us -> none  [the longest x1 41 us: per_device(): squares = lax.psum(jnp.sum(own_cols * own_cols, axis=1), ('kv', 'tp'))]
    pallas_call x0 -> x1, Pallas kernels: none -> 57.8 us  [fused(): pl.pallas_call(functools.partial(fused_kernel, cfg), out_shape=jax.ShapeD...]
    all_gather x3 -> x0, blocking collectives: 42.7 us -> none  [the longest x1 30.6 us: per_device(): head_out = lax.all_gather(own_out, 'kv', axis=0, tiled=True)]
    unnamed x6 -> x0, waiting for transfers between devices: 36.7 us -> none
    unnamed x18 -> x1, local copies, waits for them, and re-layouts: 24.3 us -> 1.28 us
    dot_general x7 -> x0, matrix products: 18.6 us -> none  [the longest x1 5.49 us: per_device(): jnp.einsum('cbkgp,bpkv->cbkgv', exp_weights, value_cache, preferred_eleme...]
    all_to_all x3 -> x0, waiting for transfers between devices: 14.3 us -> none  [the longest x1 7.09 us: per_device(): lax.all_to_all(weighted[None], 'kv', split_axis=2, concat_axis=0, tiled=T...]
  transfers between devices with their start and end apart: 7 -> 0, of which waited for: 7 -> 0; matrix products, arithmetic and copies ran while one was open for 8% -> 0% of each run, Pallas kernels for 0% -> 0%
where the time goes in v1:
time: 59.2 us; the launch traced here: 59 us
  Pallas kernels  57.8 us (98%)
  local copies, waits for them, and re-layouts  1.28 us (2%)
    pallas_call x1, Pallas kernels, fused(): pl.pallas_call(functools.partial(fused_kernel, cfg), out_shape=jax.ShapeD...  57.8 us
    unnamed x1, local copies, waits for them, and re-layouts  1.28 us

profile of v1, /device:TPU:0, one launch (start us, length us, event | category | flops | bytes accessed | tf_op | source)
XLA Modules:
  0.0 59.0 jit_solution(8825409064056294557)
XLA Ops:
  0.0 57.8 %shard_map.118 = bf16[16,128]{1,0:T(8,128)(2,1)} custom-call(bf16[16,128]{1,0:T(8,128)(2,1)} %hidden_ref.1, f32[1,512]{1,0:T(1,128)} %bitcast.7, f32[8]{0:T(128)} %lam_ref.1, f32[1,128]{1,0:T(1,128)} %bitcast.8, f32[1,128]{1,0:T(1,128)} %bitcast.9, bf16[512,1024]{1,0:T(8,128)(2,1)} %wq_hbm.1, bf16[16,2048,128]{2,1,0:T(8,128)(2,1)} %bitcast.5, ...), custom_call_target="tpu_custom_call" | custom-call | tf_op jit(solution)/shard_map/pallas_call | solution.py:351
  57.8 1.3 %copy.14 = bf16[16,128]{1,0:T(8,128)(2,1)} copy(bf16[16,128]{1,0:T(8,128)(2,1)} %shard_map.118) | data formatting | bytes 8192

commit v2 on v1

--- a/solution.py
+++ b/solution.py
@@ -24,7 +24,7 @@
     wq, kc, vc, wo, wg, wu, wd,
     xg, gsend, gainb, qs, qr, sqs, sqr, qown, qg, qall,
     acc_s, stat_s, accb, statb, accr, statr,
-    hown, hg, ps, pr, aown, ag, sq2s, sq2r, gus, gur, hid_own, hid,
+    hown, hg, projs, projr, ps, pr, ag, sq2s, sq2r, gus, gur, hid_own, hid,
     local_sem, kv_sem, send_kv, recv_kv, send_tp, recv_tp,
 ):
     n_kv, n_tp, width, head_dim, group, kv_dev = cfg
@@ -97,16 +97,17 @@
         )
 
     sent = []
+    order = sorted(range(1, n_kv), key=lambda d: (abs(2 * d - n_kv), d))
 
     def to_kv(phase, pick_src, pick_dst):
-        started = []
-        for d in range(1, n_kv):
+        started = {}
+        for d in order:
             peer = lax.rem(me + d, n_kv)
             c = kv_copy(phase, d, pick_src(d, peer), pick_dst(d))
             c.start()
-            started.append(c)
-        sent.extend(started)
-        return started
+            started[d] = c
+        sent.extend(started.values())
+        return [started[d] for d in range(1, n_kv)]
 
     def to_tp(phase, pick_src, pick_dst):
         started = []
@@ -239,29 +240,27 @@
     c_wo.wait()
     arrive(chg)
     ho = jnp.concatenate([hg[j] for j in range(heads)], axis=1)
-    proj = jnp.dot(ho, wo[...], preferred_element_type=F32).astype(BF16)
-    for t in range(n_tp):
-        ps[0, t] = proj[:, t * cols : (t + 1) * cols]
-    cp = to_tp(2, lambda d, p: ps.at[0, p], lambda d: pr.at[0, d])
-    attn = ps[0, mt].astype(F32)
-    for d, c in enumerate(cp, 1):
-        c.wait_recv()
-        attn = attn + pr[0, d].astype(F32)
-    aown[...] = (hidden_ref[...].astype(F32) + attn).astype(BF16)
-
-    ca = to_tp(3, lambda d, p: aown, lambda d: ag.at[mt])
-    ag[mt] = aown[...]
+    projs[...] = jnp.dot(ho, wo[...], preferred_element_type=F32).astype(BF16)
+    cp = to_tp(2, lambda d, p: projs, lambda d: projr.at[mt])
+    projr[mt] = projs[...]
     arrive(cgain)
     gain = jnp.concatenate([gainb[t][0:1] for t in range(n_tp)], axis=1)
-    arrive(ca)
-    af = jnp.concatenate([ag[t] for t in range(n_tp)], axis=1).astype(F32)
+    arrive(cp)
+
+    attn = projr[0].astype(F32)
+    for t in range(1, n_tp):
+        attn = attn + projr[t].astype(F32)
+    after = (xf + attn).astype(BF16)
+    for t in range(n_tp):
+        ag[t] = after[:, t * cols : (t + 1) * cols]
+    af = after.astype(F32)
     mixin = (af * gain).astype(BF16)
     sq2s[...] = pack_rows(jnp.sum(af * af, axis=1, keepdims=True))
     csq2 = to_kv(6, lambda d, p: sq2s, lambda d: sq2r.at[d])
     c_wg.wait()
     c_wu.wait()
-    cgu = []
-    for d in list(range(1, n_kv)) + [0]:
+    cgu = {}
+    for d in order + [0]:
         peer = lax.rem(me + d, n_kv)
         at = pl.ds(pl.multiple_of(peer * piece, LANES), piece)
         gp = jnp.dot(mixin, wg[:, at], preferred_element_type=F32)
@@ -273,14 +272,14 @@
             gus[d, 1] = up.astype(BF16)
             c = kv_copy(7, d, gus.at[d], gur.at[d])
             c.start()
-            cgu.append(c)
-    sent.extend(cgu)
+            cgu[d] = c
+    sent.extend(cgu.values())
     arrive(csq2)
     sq = sq2s[...]
     for d in range(1, n_kv):
         sq = sq + sq2r[d]
     scale2 = lax.rsqrt(unpack_rows(sq) / width + eps)
-    for d, c in enumerate(cgu, 1):
+    for d, c in sorted(cgu.items()):
         c.wait_recv()
         gate_sum = gate_sum + gur[d, 0].astype(F32)
         up_sum = up_sum + gur[d, 1].astype(F32)
@@ -298,13 +297,13 @@
         down = down + jnp.dot(hid[src], wd[at, :], preferred_element_type=F32)
     downb = down.astype(BF16)
     for t in range(n_tp):
-        ps[1, t] = downb[:, t * cols : (t + 1) * cols]
-    cd = to_tp(4, lambda d, p: ps.at[1, p], lambda d: pr.at[1, d])
-    mix = ps[1, mt].astype(F32)
+        ps[t] = downb[:, t * cols : (t + 1) * cols]
+    cd = to_tp(3, lambda d, p: ps.at[p], lambda d: pr.at[d])
+    mix = ps[mt].astype(F32)
     for d, c in enumerate(cd, 1):
         c.wait_recv()
-        mix = mix + pr[1, d].astype(F32)
-    out_ref[...] = (aown[...].astype(F32) + mix).astype(BF16)
+        mix = mix + pr[d].astype(F32)
+    out_ref[...] = (ag[mt].astype(F32) + mix).astype(BF16)
     for c in sent:
         c.wait_send()
 
@@ -335,14 +334,15 @@
         V((heads, 2 * batch, hw), BF16), V((heads, batch, LANES), F32),
         V((n_kv, 2 * batch, hw), BF16), V((n_kv, batch, LANES), F32),
         V((batch, hw), BF16), V((heads, batch, hw), BF16),
-        V((2, n_tp, batch, cols), BF16), V((2, n_tp, batch, cols), BF16),
-        V((batch, cols), BF16), V((n_tp, batch, cols), BF16),
+        V((batch, block), BF16), V((n_tp, batch, block), BF16),
+        V((n_tp, batch, cols), BF16), V((n_tp, batch, cols), BF16),
+        V((n_tp, batch, cols), BF16),
         V((half, LANES), F32), V((n_kv, half, LANES), F32),
         V((n_kv, 2, batch, piece), BF16), V((n_kv, 2, batch, piece), BF16),
         V((batch, piece), BF16), V((n_kv, batch, piece), BF16),
         pltpu.SemaphoreType.DMA((5,)), pltpu.SemaphoreType.DMA((2, CHUNKS)),
         pltpu.SemaphoreType.DMA((9, n_kv)), pltpu.SemaphoreType.DMA((9, n_kv)),
-        pltpu.SemaphoreType.DMA((5, n_tp)), pltpu.SemaphoreType.DMA((5, n_tp)),
+        pltpu.SemaphoreType.DMA((4, n_tp)), pltpu.SemaphoreType.DMA((4, n_tp)),
     ]
     vmem = pl.BlockSpec(memory_space=pltpu.VMEM)
     smem = pl.BlockSpec(memory_space=pltpu.SMEM)

time: 59.2 us -> 57.3 us (0.968)
  Pallas kernels: 57.8 us -> 55.8 us
    pallas_call x1, Pallas kernels: 57.8 us -> 55.8 us  [fused(): pl.pallas_call(functools.partial(fused_kernel, cfg), out_shape=jax.ShapeD...]
where the time goes in v2:
time: 57.3 us; the launch traced here: 57.1 us
  Pallas kernels  55.8 us (97%)
  local copies, waits for them, and re-layouts  1.28 us (2%)
    pallas_call x1, Pallas kernels, fused(): pl.pallas_call(functools.partial(fused_kernel, cfg), out_shape=jax.ShapeD...  55.8 us
    unnamed x1, local copies, waits for them, and re-layouts  1.28 us

profile of v2, /device:TPU:0, one launch (start us, length us, event | category | flops | bytes accessed | tf_op | source)
XLA Modules:
  0.0 57.1 jit_solution(14471921458825520337)
XLA Ops:
  0.0 55.8 %shard_map.118 = bf16[16,128]{1,0:T(8,128)(2,1)} custom-call(bf16[16,128]{1,0:T(8,128)(2,1)} %hidden_ref.1, f32[1,512]{1,0:T(1,128)} %bitcast.7, f32[8]{0:T(128)} %lam_ref.1, f32[1,128]{1,0:T(1,128)} %bitcast.8, f32[1,128]{1,0:T(1,128)} %bitcast.9, bf16[512,1024]{1,0:T(8,128)(2,1)} %wq_hbm.1, bf16[16,2048,128]{2,1,0:T(8,128)(2,1)} %bitcast.5, ...), custom_call_target="tpu_custom_call" | custom-call | tf_op jit(solution)/shard_map/pallas_call | solution.py:351
  55.8 1.3 %copy.14 = bf16[16,128]{1,0:T(8,128)(2,1)} copy(bf16[16,128]{1,0:T(8,128)(2,1)} %shard_map.118) | data formatting | bytes 8192
